TPU v7x, 512 devices: a 8x2x16 block of a 8x8x16 slice. The times are simulated.
512 devices in a mesh: grp: 2 (over y), dp: 8 (over x), kv: 16 (over z), tp: 2 (over core).
Axes of the slice: x: 8, y: 2, z: 16, core: 2. Of those that a mesh axis runs over, the one named last changes fastest.
The devices are a block of a 8x8x16 slice.
Arguments:
- tokens: bfloat16 [384, 4, 4096], P(('grp', 'dp'), None, ('kv', 'tp')), parts along dimension 0, may hold values from -6 to 6
- norm_gain: float32 [4096], replicated, may hold values from 0.1 to 1.9
- w_query: bfloat16 [16, 128, 4096], P('kv', 'tp'), may hold values from -0.09375 to 0.09375
- w_key: bfloat16 [16, 128, 4096], P('kv', 'tp'), may hold values from -0.09375 to 0.09375
- w_value: bfloat16 [16, 128, 4096], P('kv', 'tp'), may hold values from -0.09375 to 0.09375
- w_gate: bfloat16 [16, 128, 4096], P('kv', 'tp'), may hold values from -0.09375 to 0.09375
- w_decay: bfloat16 [4096, 16], replicated, may hold values from -0.09375 to 0.09375
- w_beta: bfloat16 [4096, 16], replicated, may hold values from -0.09375 to 0.09375
- decay_rate: float32 [16], P('kv'), may hold values from 0.02 to 1
- head_gain: float32 [128], P('tp'), may hold values from 0.1 to 1.9
- w_out: bfloat16 [16, 128, 4096], P('kv', 'tp'), may hold values from -0.1875 to 0.1875
- state: float32 [384, 16, 128, 128], P(('grp', 'dp'), 'kv', 'tp'), parts along dimension 0, may hold values from -6 to 6
- prev_keys: bfloat16 [384, 4, 16, 128], P(('grp', 'dp'), None, 'kv'), parts along dimension 0, may hold values from -6 to 6
- prev_values: bfloat16 [384, 4, 16, 128], P(('grp', 'dp'), None, 'kv', 'tp'), parts along dimension 0, may hold values from -6 to 6
- prev_decay: float32 [384, 4, 16], P(('grp', 'dp'), None, 'kv'), parts along dimension 0, may hold values from 0.01 to 1
- prev_beta: float32 [384, 4, 16], P(('grp', 'dp'), None, 'kv'), parts along dimension 0, may hold values from 0.05 to 1
- accepted: int32 [384], P(('grp', 'dp')), parts along dimension 0, may hold values from 0 to 4
Outputs:
- mixed: bfloat16 [384, 4, 4096], P(('grp', 'dp'), None, ('kv', 'tp')), parts along dimension 0
- committed: float32 [384, 16, 128, 128], P(('grp', 'dp'), 'kv', 'tp'), parts along dimension 0
There are 2 independent parts, one for each index of `grp`. A program takes and returns all parts, laid end to end along the dimension named above; an argument that names none is the same for every part. Nothing has to cross between parts.
All inputs are finite; a program needn't handle non-finite values.
Results may differ from a plain program's by a relative error of at most 0.015.
Values may be sent and summed in bfloat16 or wider, within the bound.
No kernel may reach another device: no remote copies, remote signals or barrier semaphores. Data moves between devices by JAX's collectives and lax.ppermute only.
A program may use at most 64 MiB of HBM per device.

v0:
```python
import jax
import jax.numpy as jnp
from jax import lax
from jax.experimental import pallas as pl
from jax.experimental.pallas import tpu as pltpu
from jax.sharding import PartitionSpec as P


EPS = 1e-06
F32 = jnp.float32
BF16 = jnp.bfloat16
SWAP = [(0, 1), (1, 0)]


def mm(a, b, dims=((1,), (0,))):
    return lax.dot_general(
        a.astype(BF16), b.astype(BF16), (dims, ((), ())), preferred_element_type=F32
    )


NT = ((1,), (1,))


def high(a, b):
    return lax.dot_general(
        a, b, (((1,), (0,)), ((), ())), precision=lax.Precision.HIGHEST, preferred_element_type=F32
    )


def silu(x):
    return x / (1.0 + jnp.exp(-x))


def turned(x):
    n = x.shape[1]
    eye = lax.broadcasted_iota(jnp.int32, (n, n), 0) == lax.broadcasted_iota(jnp.int32, (n, n), 1)
    return mm(jnp.where(eye, 1.0, 0.0), x, NT)


def decays(d_row, steps):
    n = d_row.shape[1]
    shift = steps.bit_length() - 1
    i = lax.broadcasted_iota(jnp.int32, (n, n), 0)
    r = lax.broadcasted_iota(jnp.int32, (n, n), 1)
    same = (i >> shift) == (r >> shift)
    upto = same & (i <= r)
    before = same & (i < r)
    d_col = jnp.sum(jnp.where(i == r, d_row, 0.0), axis=1, keepdims=True)
    g_row = jnp.sum(jnp.where(upto, d_col, 0.0), axis=0, keepdims=True)
    g_col = jnp.sum(jnp.where(i == r, g_row, 0.0), axis=1, keepdims=True)
    between = jnp.where(upto, jnp.exp(jnp.where(upto, g_row - g_col, 0.0)), 0.0)
    last = jnp.sum(jnp.where(same & ((i & (steps - 1)) == steps - 1), g_col, 0.0), axis=0, keepdims=True)
    return g_row, g_col, last, between, before


def inverse(n):
    eye = lax.broadcasted_iota(jnp.int32, n.shape, 0) == lax.broadcasted_iota(jnp.int32, n.shape, 1)
    square = high(n, n)
    return jnp.where(eye, 1.0, 0.0) - n + square - high(n, square)


def own_products(states, keys_t, seqs, steps):
    product = mm(states, keys_t)
    rows, n = product.shape[0] // seqs, product.shape[1]
    shift = steps.bit_length() - 1
    seq_of = lax.broadcasted_iota(jnp.int32, (rows, n), 1) >> shift
    total = jnp.zeros((rows, n), F32)
    for s in range(seqs):
        total = total + jnp.where(seq_of == s, product[s * rows : (s + 1) * rows], 0.0)
    return total


def commit_kernel(
    state_hbm, keys_hbm, values_hbm, decay_hbm, beta_hbm, accepted_hbm, hg_hbm, wq_ref, wk_ref, wv_ref, wg_ref, wo_ref,
    out_ref, pack_ref, state_ref, keys_ref, values_ref, decay_ref, beta_ref, accepted_ref, hg_ref, weights, states, sent, sems,
):
    seqs, rows, width = state_ref.shape
    steps = decay_ref.shape[0]
    n = seqs * steps
    shift = steps.bit_length() - 1
    count = 5
    loads = [
        pltpu.make_async_copy(w, weights.at[k * rows : (k + 1) * rows], sems.at[k])
        for k, w in enumerate((wq_ref, wk_ref, wv_ref, wg_ref, wo_ref))
    ]
    small = [
        pltpu.make_async_copy(a, b, sems.at[count + 3 + k])
        for k, (a, b) in enumerate(
            (
                (keys_hbm, keys_ref),
                (decay_hbm, decay_ref),
                (beta_hbm, beta_ref),
                (accepted_hbm, accepted_ref),
                (values_hbm, values_ref),
                (hg_hbm, hg_ref),
                (state_hbm, state_ref),
            )
        )
    ]
    for load in small + loads:
        load.start()
    for load in small[:-1]:
        load.wait()
    keys = keys_ref[...].astype(F32)
    keys = keys * lax.rsqrt(jnp.sum(keys * keys, axis=-1, keepdims=True) + EPS)
    keys_t = turned_f32(keys)
    step_of = lax.broadcasted_iota(jnp.int32, (steps, n), 1) & (steps - 1)
    own_step = step_of == lax.broadcasted_iota(jnp.int32, (steps, n), 0)
    owner = lax.broadcasted_iota(jnp.int32, (seqs, n), 1) >> shift
    spread = jnp.where(owner == lax.broadcasted_iota(jnp.int32, (seqs, n), 0), 1.0, 0.0)
    taken = high(accepted_ref[...].astype(F32), spread)
    live = jnp.where(step_of[0:1].astype(F32) < taken - 0.5, 1.0, 0.0)
    d_row = -jnp.sum(jnp.where(own_step, high(decay_ref[...], spread), 0.0), axis=0, keepdims=True) * live
    b_row = jnp.sum(jnp.where(own_step, high(beta_ref[...], spread), 0.0), axis=0, keepdims=True) * live
    g_row, g_col, last, between, before = decays(d_row, steps)
    gram = mm(keys, keys, NT)
    nil = jnp.where(before, between * gram * b_row, 0.0)
    back = inverse(nil)
    values_t = turned(values_ref[...])
    small[-1].wait()
    state = state_ref[...]
    known = own_products(state.reshape(seqs * rows, width), keys_t, seqs, steps)
    stores = []
    for k, load in enumerate(loads):
        at = slice(k * rows, (k + 1) * rows)
        load.wait()
        stores.append(pltpu.make_async_copy(weights.at[at], pack_ref.at[at], sems.at[count + 10 + k]))
        stores[-1].start()
    u = high(b_row * (values_t - jnp.exp(g_row) * known), back) * jnp.exp(last - g_row)
    seq_of = lax.broadcasted_iota(jnp.int32, (rows, n), 1) >> shift
    spread_u = jnp.concatenate([jnp.where(seq_of == s, u, 0.0).astype(BF16) for s in range(seqs)], axis=0)
    update = mm(spread_u, keys)
    kept = jnp.broadcast_to(jnp.exp(g_col), (n, width))
    for s in range(seqs):
        at = s * steps + steps - 1
        states[s] = state[s] * kept[at : at + 1, :] + update[s * rows : (s + 1) * rows]
    half = seqs // 2
    tp = lax.axis_index("tp")
    for s in range(half):
        sent[:, s * width : (s + 1) * width] = states[(1 - tp) * half + s].astype(BF16)
    pieces, rest = [], jnp.concatenate([hg_ref[...], jnp.zeros((1, width - rows), F32)], axis=1)
    for _ in range(3):
        pieces.append(rest.astype(BF16).astype(F32))
        rest = rest - pieces[-1]
    pieces.append(jnp.zeros((rows - 3, width), F32))
    sent[:, half * width :] = jnp.concatenate(pieces, axis=0).astype(BF16)
    stores.append(pltpu.make_async_copy(states, out_ref, sems.at[count + 1]))
    stores[-1].start()
    columns = (half + 1) * width
    stores.append(pltpu.make_async_copy(sent, pack_ref.at[count * rows :, :columns], sems.at[count + 2]))
    stores[-1].start()
    for store in stores:
        store.wait()


def turned_f32(x):
    return turned(x.astype(BF16))


def layer_kernel(
    x_ref, gain_ref, wq_ref, wk_ref, wv_ref, wg_ref, decay_ref, beta_ref, rate_ref, hg_ref, committed_hbm, wo_ref, pack_hbm,
    out_ref, same_hbm, keep_ref, pack_ref, sems,
):
    _, blocks, all_rows, lanes = x_ref.shape
    n = all_rows // 2
    seqs, rows, width = keep_ref.shape
    steps = n // seqs
    heads = decay_ref.shape[0]
    tp = lax.axis_index("tp")
    head = lax.axis_index("kv")
    features = blocks * 2 * lanes
    copies = []

    def fetch(src, dst):
        copies.append(pltpu.make_async_copy(src, dst, sems.at[len(copies)]))
        copies[-1].start()
        return copies[-1]

    cuts = 4
    cut = features // cuts
    weight_copies = [
        fetch(pack_hbm.at[: 4 * rows, c * cut : (c + 1) * cut], pack_ref.at[: 4 * rows, c * cut : (c + 1) * cut])
        for c in range(cuts)
    ]
    columns = (seqs + 1) * width
    state_copies = [
        fetch(same_hbm.at[pl.ds(tp * seqs, seqs)], keep_ref),
        fetch(pack_hbm.at[5 * rows :, :columns], pack_ref.at[5 * rows :, :columns]),
    ]
    out_copy = fetch(pack_hbm.at[4 * rows : 5 * rows], pack_ref.at[4 * rows : 5 * rows])
    own_rows = pl.ds(pl.multiple_of(tp * n, n), n)
    squares = jnp.zeros((n, lanes), F32)
    for b in range(blocks):
        for c in range(2):
            part = x_ref[c, b, own_rows, :].astype(F32)
            squares = squares + part * part
    scale = lax.rsqrt(jnp.sum(squares, axis=-1, keepdims=True) / features + EPS)
    mine = jnp.zeros((4 * rows, n), F32)
    others = jnp.zeros((4 * rows, n), F32)
    gates = jnp.zeros((2 * heads, n), F32)
    for b in range(blocks):
        if b % (blocks // cuts) == 0:
            weight_copies[b // (blocks // cuts)].wait()
        at = slice(b * 2 * lanes, (b + 1) * 2 * lanes)
        pair = jnp.concatenate([x_ref[c, b, own_rows, :] for c in range(2)], axis=1).astype(F32)
        gain = jnp.concatenate([gain_ref[2 * b : 2 * b + 1, :], gain_ref[2 * b + 1 : 2 * b + 2, :]], axis=1)
        normed = (pair * scale * gain).astype(BF16)
        w = jnp.concatenate([r[:, at] for r in (wq_ref, wk_ref, wv_ref, wg_ref)], axis=0)
        mine = mine + mm(w, normed, NT)
        others = others + mm(pack_ref[: 4 * rows, at], normed, NT)
        w = jnp.concatenate([decay_ref[:, at], beta_ref[:, at]], axis=0)
        gates = gates + mm(w, normed, NT)
    for copy in state_copies:
        copy.wait()
    mine = mine.astype(BF16).astype(F32)
    others = others.astype(BF16).astype(F32)

    def in_order(k):
        a, b = mine[k * rows : (k + 1) * rows], others[k * rows : (k + 1) * rows]
        return jnp.where(tp == 0, jnp.concatenate([a, b], axis=0), jnp.concatenate([b, a], axis=0))

    def own_first(k):
        return jnp.concatenate([mine[k * rows : (k + 1) * rows], others[k * rows : (k + 1) * rows]], axis=0)

    def unit(u):
        return u * lax.rsqrt(jnp.sum(u * u, axis=0, keepdims=True) + EPS)

    query = unit(silu(in_order(0))) * width ** (-0.5)
    key = unit(silu(in_order(1)))
    value = silu(own_first(2))
    gate = silu(own_first(3))
    at_head = lax.broadcasted_iota(jnp.int32, (heads, n), 0) == head
    decay_pre = jnp.sum(jnp.where(at_head, gates[:heads], 0.0), axis=0, keepdims=True)
    beta_pre = jnp.sum(jnp.where(at_head, gates[heads:], 0.0), axis=0, keepdims=True)
    softplus = jnp.maximum(decay_pre, 0.0) + jnp.log1p(jnp.exp(-jnp.abs(decay_pre)))
    d_row = -rate_ref[0] * softplus
    b_row = 1.0 / (1.0 + jnp.exp(-beta_pre))
    g_row, _, _, between, before = decays(d_row, steps)

    kept = keep_ref[...].reshape(seqs * rows, width).astype(BF16)
    got = jnp.concatenate([pack_ref[5 * rows :, s * width : (s + 1) * width] for s in range(seqs)], axis=0)

    def from_states(u):
        return jnp.concatenate([own_products(c, u, seqs, steps) for c in (kept, got)], axis=0)

    key_rows = turned_f32(key)
    nil = jnp.where(before, between * mm(key_rows, key) * b_row, 0.0)
    back = inverse(nil)
    u = high(b_row * (value - jnp.exp(g_row) * from_states(key)), back)
    o = jnp.exp(g_row) * from_states(query) + high(u, between * mm(key_rows, query))
    norm = lax.rsqrt(jnp.mean(o * o, axis=0, keepdims=True) + EPS)
    eye = lax.broadcasted_iota(jnp.int32, (rows, rows), 0) == lax.broadcasted_iota(jnp.int32, (rows, rows), 1)
    pieces = pack_ref[5 * rows :, seqs * width : (seqs + 1) * width].astype(F32)[:3, :rows]
    other_gain = pieces[0:1] + pieces[1:2] + pieces[2:3]
    head_gain = jnp.concatenate(
        [jnp.sum(jnp.where(eye, h, 0.0), axis=1, keepdims=True) for h in (hg_ref[...], other_gain)], axis=0
    )
    scaled = turned_f32(o * norm * head_gain * gate).astype(BF16)
    out_copy.wait()
    columns = out_ref.shape[2]
    for b in range(blocks):
        at = slice(b * columns, (b + 1) * columns)
        w = jnp.concatenate([wo_ref[:, at], pack_ref[4 * rows : 5 * rows, at]], axis=0)
        out_ref[b] = mm(scaled, w).astype(BF16)


HBM = pl.BlockSpec(memory_space=pltpu.HBM)
ANY = pl.BlockSpec(memory_space=pl.ANY)
VMEM = pl.BlockSpec(memory_space=pltpu.VMEM)
SMEM = pl.BlockSpec(memory_space=pltpu.SMEM)


def local(
    tokens,
    norm_gain,
    w_query,
    w_key,
    w_value,
    w_gate,
    w_decay,
    w_beta,
    decay_rate,
    head_gain,
    w_out,
    state,
    prev_keys,
    prev_values,
    prev_decay,
    prev_beta,
    accepted,
):
    seqs, steps, lanes = tokens.shape
    half = seqs // 2
    n = half * steps
    rows, features = w_query.shape[1:]
    width = state.shape[-1]
    kv = lax.axis_size("kv")
    tp = lax.axis_index("tp")

    copies = jnp.broadcast_to(tokens.reshape(1, seqs * steps, lanes), (kv, seqs * steps, lanes))
    ours = lax.all_to_all(copies, "kv", split_axis=0, concat_axis=0, tiled=True)
    weights = [w.reshape(rows, features) for w in (w_query, w_key, w_value, w_gate)]
    w_own = w_out.reshape(rows, features)
    gain = head_gain.reshape(1, rows)
    commit = pl.pallas_call(
        commit_kernel,
        out_shape=(
            jax.ShapeDtypeStruct((seqs, rows, width), F32),
            jax.ShapeDtypeStruct((6 * rows, features), BF16),
        ),
        in_specs=[HBM] * 12,
        out_specs=(HBM, HBM),
        scratch_shapes=[
            pltpu.VMEM((seqs, rows, width), F32),
            pltpu.VMEM((seqs * steps, width), BF16),
            pltpu.VMEM((seqs * steps, rows), BF16),
            pltpu.VMEM((steps, seqs), F32),
            pltpu.VMEM((steps, seqs), F32),
            pltpu.VMEM((1, seqs), jnp.int32),
            pltpu.VMEM((1, rows), F32),
            pltpu.VMEM((5 * rows, features), BF16),
            pltpu.VMEM((seqs, rows, width), F32),
            pltpu.VMEM((rows, (half + 1) * width), BF16),
            pltpu.SemaphoreType.DMA((20,)),
        ],
        cost_estimate=pl.CostEstimate(flops=2 * 10**9, bytes_accessed=8 * 10**6, transcendentals=0),
        name="commit",
    )
    committed, pack = commit(
        state.reshape(seqs, rows, width),
        prev_keys.reshape(seqs * steps, width),
        prev_values.reshape(seqs * steps, rows),
        prev_decay[:, :, 0].T,
        prev_beta[:, :, 0].T,
        accepted.reshape(1, seqs),
        gain,
        *weights,
        w_own,
    )
    pack = lax.ppermute(pack, "tp", SWAP)
    gathered = lax.all_gather(ours, "tp", axis=0)
    columns = features // kv
    partial, committed = pl.pallas_call(
        layer_kernel,
        out_shape=(
            jax.ShapeDtypeStruct((kv, n, columns), BF16),
            jax.ShapeDtypeStruct((seqs, rows, width), F32),
        ),
        input_output_aliases={10: 1},
        in_specs=[VMEM] * 8 + [SMEM, VMEM, HBM, VMEM, HBM],
        out_specs=(VMEM, HBM),
        scratch_shapes=[
            pltpu.VMEM((half, rows, width), F32),
            pltpu.VMEM((6 * rows, features), BF16),
            pltpu.SemaphoreType.DMA((8,)),
        ],
        cost_estimate=pl.CostEstimate(flops=10**9, bytes_accessed=6 * 10**6, transcendentals=0),
        compiler_params=pltpu.CompilerParams(vmem_limit_bytes=48 * 2**20),
        name="layer",
    )(
        gathered,
        norm_gain.reshape(features // lanes, lanes),
        *weights,
        w_decay.T,
        w_beta.T,
        decay_rate,
        gain,
        committed,
        w_own,
        pack,
    )
    parts = lax.all_to_all(partial, "kv", split_axis=0, concat_axis=0, tiled=True)
    total = parts.astype(F32).sum(axis=0).astype(BF16)
    mixed = lax.dynamic_slice_in_dim(lax.all_gather(total, "tp", axis=0), tp * lanes, lanes, 2)
    return mixed.reshape(seqs, steps, lanes), committed.reshape(state.shape)


def solution(mesh):
    in_specs = (
        P(("grp", "dp"), None, ("kv", "tp")),
        P(),
        P("kv", "tp", None),
        P("kv", "tp", None),
        P("kv", "tp", None),
        P("kv", "tp", None),
        P(),
        P(),
        P("kv"),
        P("tp"),
        P("kv", "tp", None),
        P(("grp", "dp"), "kv", "tp", None),
        P(("grp", "dp"), None, "kv", None),
        P(("grp", "dp"), None, "kv", "tp"),
        P(("grp", "dp"), None, "kv"),
        P(("grp", "dp"), None, "kv"),
        P(("grp", "dp")),
    )
    out_specs = (P(("grp", "dp"), None, ("kv", "tp")), P(("grp", "dp"), "kv", "tp", None))
    return jax.shard_map(local, mesh=mesh, in_specs=in_specs, out_specs=out_specs, check_vma=False)
```

profile of v0, /device:TPU:65, one launch (start us, length us, event | category | flops | bytes accessed | tf_op | source)
XLA Modules:
  0.0 117.4 jit_solution(11094704460707761429)
XLA Ops:
  0.6 0.0 copy-start.9
  0.6 0.0 copy-start
  0.7 0.0 copy-start.1
  0.7 0.0 copy-start.2
  0.7 0.0 copy-start.3
  0.7 0.0 copy-start.4
  0.7 0.0 copy-start.5
  0.7 0.0 copy-start.6
  0.7 0.0 copy-start.7
  0.7 0.0 copy-start.8
  0.7 4.0 %commit.1 = (f32[24,64,128]{2,1,0:T(8,128)}, bf16[384,4096]{1,0:T(8,128)(2,1)}) custom-call(f32[24,64,128]{2,1,0:T(8,128)} %bitcast.46, bf16[96,128]{1,0:T(8,128)(2,1)} %bitcast.47, bf16[96,64]{1,0:T(8,128)(2,1)} %bitcast.48, f32[4,24]{1,0:T(4,128)} %bitcast.49, f32[4,24]{1,0:T(4,128)} %bitcast.50, s32[1,24]{1,0:T(1,128)} %bitcast.51, f32[1,64]{1,0:T(1,128)} %bitcast.40, ...), custom_call_target="tpu_custom_call" | custom-call | flops 2000000000 | bytes 8000000 | tf_op jit(solution)/shard_map/commit/pallas_call | solution.py:329
  4.8 43.4 %collective-permute-start = (bf16[384,4096]{1,0:T(8,128)(2,1)}, bf16[384,4096]{1,0:T(8,128)(2,1)}, u32[]{:S(2)}, u32[]{:S(2)}) collective-permute-start(bf16[384,4096]{1,0:T(8,128)(2,1)} %get-tuple-element.7), channel_id=1, source_target_pairs={{0,1},{1,0},{2,3},{3,2},{4,5},{5,4},{6,7},{7,6},{8,9},{9,8},{10,11... | collective-permute-start | bytes 9437192 | tf_op jit(solution)/shard_map/ppermute | solution.py:340
  48.2 0.0 copy-done.9
  48.2 0.8 broadcast_in_dim.8
  49.0 4.0 %all-to-all-start = ((bf16[16,96,128]{2,1,0:T(8,128)(2,1)}), bf16[16,96,128]{2,1,0:T(8,128)(2,1)S(1)}, u32[]{:S(2)}, u32[]{:S(2)}) async-start(bf16[16,96,128]{2,1,0:T(8,128)(2,1)} %broadcast_in_dim.8), calls=%async_computation | async-start | bytes 786432 | tf_op jit(solution)/shard_map/all_to_all | solution.py:301
  53.6 19.4 %all-to-all-done = bf16[16,96,128]{2,1,0:T(8,128)(2,1)S(1)} async-done(((bf16[16,96,128]{2,1,0:T(8,128)(2,1)}), bf16[16,96,128]{2,1,0:T(8,128)(2,1)S(1)}, u32[]{:S(2)}, u32[]{:S(2)}) %all-to-all-start) | async-done | bytes 393248 | tf_op jit(solution)/shard_map/all_to_all | solution.py:301
  73.1 6.1 %all-gather = bf16[32,96,128]{2,1,0:T(8,128)(2,1)S(1)} all-gather(bf16[16,96,128]{2,1,0:T(8,128)(2,1)S(1)} %all-to-all-done), channel_id=2, replica_groups=mesh['grp'=2,'dp'=8,'kv'=16,'tp'=2] {'tp'}, dimensions={0}, use_global_device_ids=true | all-gather | bytes 1179648 | tf_op jit(solution)/shard_map/all_gather | solution.py:341
  79.2 0.0 collective-permute-done.pack_hbm
  79.2 0.0 copy-done
  79.2 0.0 copy-done.1
  79.2 0.0 copy-done.3
  79.2 0.0 copy-done.4
  79.2 0.0 copy-done.5
  79.2 0.0 copy-done.6
  79.2 0.0 copy-done.7
  79.2 0.0 copy-done.8
  79.2 5.1 %layer.1 = (bf16[16,48,256]{2,1,0:T(8,128)(2,1)}, f32[24,64,128]{2,1,0:T(8,128)}) custom-call(bf16[2,16,96,128]{3,2,1,0:T(8,128)(2,1)S(1)} %bitcast.26, f32[32,128]{1,0:T(8,128)S(1)} %bitcast.39, bf16[64,4096]{1,0:T(8,128)(2,1)S(1)} %bitcast.28, bf16[64,4096]{1,0:T(8,128)(2,1)S(1)} %bitcast.30, ...), custom_call_target="tpu_custom_call", output_to_operand_aliasing={{1}: (10, {})} | custom-call | flops 1000000000 | bytes 6000000 | tf_op jit(solution)/shard_map/layer/pallas_call | solution.py:343
  84.3 6.1 %all-to-all-start.1 = ((bf16[16,48,256]{2,1,0:T(8,128)(2,1)}), bf16[16,48,256]{2,1,0:T(8,128)(2,1)S(1)}, u32[]{:S(2)}, u32[]{:S(2)}) async-start(bf16[16,48,256]{2,1,0:T(8,128)(2,1)} %get-tuple-element.8), calls=%async_computation.1 | async-start | bytes 786432 | tf_op jit(solution)/shard_map/all_to_all | solution.py:372
  90.5 17.3 %all-to-all-done.1 = bf16[16,48,256]{2,1,0:T(8,128)(2,1)S(1)} async-done(((bf16[16,48,256]{2,1,0:T(8,128)(2,1)}), bf16[16,48,256]{2,1,0:T(8,128)(2,1)S(1)}, u32[]{:S(2)}, u32[]{:S(2)}) %all-to-all-start.1) | async-done | bytes 393248 | tf_op jit(solution)/shard_map/all_to_all | solution.py:372
  107.8 0.1 reduce_sum.12
  107.8 9.0 %all-gather.1 = bf16[96,256]{1,0:T(8,128)(2,1)S(1)} all-gather(bf16[48,256]{1,0:T(8,128)(2,1)S(1)} %reduce_sum.12), channel_id=3, replica_groups=mesh['grp'=2,'dp'=8,'kv'=16,'tp'=2] {'tp'}, dimensions={0}, use_global_device_ids=true | all-gather | bytes 73728 | tf_op jit(solution)/shard_map/all_gather | solution.py:374
  116.8 0.6 constant_dynamic-slice_fusion
  (1 shorter events, 0.0 us)
Async XLA Ops:
  0.6 47.5 %copy-start.9 = (bf16[24,4,128]{2,1,0:T(4,128)(2,1)S(1)}, bf16[24,4,128]{2,1,0:T(4,128)(2,1)}, u32[]{:S(2)}) copy-start(bf16[24,4,128]{2,1,0:T(4,128)(2,1)} %param.17) | copy-start | bytes 73732
  0.6 78.5 %copy-start = (bf16[1,64,4096]{2,1,0:T(8,128)(2,1)S(1)}, bf16[1,64,4096]{2,1,0:T(8,128)(2,1)}, u32[]{:S(2)}) copy-start(bf16[1,64,4096]{2,1,0:T(8,128)(2,1)} %param.19) | copy-start | bytes 1572868
  0.7 78.5 %copy-start.1 = (bf16[1,64,4096]{2,1,0:T(8,128)(2,1)S(1)}, bf16[1,64,4096]{2,1,0:T(8,128)(2,1)}, u32[]{:S(2)}) copy-start(bf16[1,64,4096]{2,1,0:T(8,128)(2,1)} %param.20) | copy-start | bytes 1572868
  0.7 78.5 %copy-start.2 = (bf16[1,64,4096]{2,1,0:T(8,128)(2,1)S(1)}, bf16[1,64,4096]{2,1,0:T(8,128)(2,1)}, u32[]{:S(2)}) copy-start(bf16[1,64,4096]{2,1,0:T(8,128)(2,1)} %param.21) | copy-start | bytes 1572868
  0.7 78.5 %copy-start.3 = (bf16[1,64,4096]{2,1,0:T(8,128)(2,1)S(1)}, bf16[1,64,4096]{2,1,0:T(8,128)(2,1)}, u32[]{:S(2)}) copy-start(bf16[1,64,4096]{2,1,0:T(8,128)(2,1)} %param.22) | copy-start | bytes 1572868
  0.7 78.5 %copy-start.4 = (bf16[1,64,4096]{2,1,0:T(8,128)(2,1)S(1)}, bf16[1,64,4096]{2,1,0:T(8,128)(2,1)}, u32[]{:S(2)}) copy-start(bf16[1,64,4096]{2,1,0:T(8,128)(2,1)} %param.27) | copy-start | bytes 1572868
  0.7 78.5 %copy-start.5 = (bf16[4096,16]{0,1:T(8,128)(2,1)S(1)}, bf16[4096,16]{0,1:T(8,128)(2,1)}, u32[]{:S(2)}) copy-start(bf16[4096,16]{0,1:T(8,128)(2,1)} %param.23) | copy-start | bytes 393220
  0.7 78.5 %copy-start.6 = (bf16[4096,16]{0,1:T(8,128)(2,1)S(1)}, bf16[4096,16]{0,1:T(8,128)(2,1)}, u32[]{:S(2)}) copy-start(bf16[4096,16]{0,1:T(8,128)(2,1)} %param.24) | copy-start | bytes 393220
  0.7 78.5 %copy-start.7 = (f32[4096]{0:T(1024)S(1)}, f32[4096]{0:T(1024)}, u32[]{:S(2)}) copy-start(f32[4096]{0:T(1024)} %param.18) | copy-start | bytes 49156
  0.7 78.5 %copy-start.8 = (f32[64]{0:T(128)S(1)}, f32[64]{0:T(128)}, u32[]{:S(2)}) copy-start(f32[64]{0:T(128)} %param.26) | copy-start | bytes 772
  4.8 74.4 %collective-permute-start = (bf16[384,4096]{1,0:T(8,128)(2,1)}, bf16[384,4096]{1,0:T(8,128)(2,1)}, u32[]{:S(2)}, u32[]{:S(2)}) collective-permute-start(bf16[384,4096]{1,0:T(8,128)(2,1)} %get-tuple-element.7), channel_id=1, source_target_pairs={{0,1},{1,0},{2,3},{3,2},{4,5},{5,4},{6,7},{7,6},{8,9},{9,8},{10,11... | collective-permute-start | bytes 9437192 | tf_op jit(solution)/shard_map/ppermute | solution.py:340
  49.0 24.1 %all-to-all-start = ((bf16[16,96,128]{2,1,0:T(8,128)(2,1)}), bf16[16,96,128]{2,1,0:T(8,128)(2,1)S(1)}, u32[]{:S(2)}, u32[]{:S(2)}) async-start(bf16[16,96,128]{2,1,0:T(8,128)(2,1)} %broadcast_in_dim.8), calls=%async_computation | async-start | bytes 786432 | tf_op jit(solution)/shard_map/all_to_all | solution.py:301
  84.3 23.4 %all-to-all-start.1 = ((bf16[16,48,256]{2,1,0:T(8,128)(2,1)}), bf16[16,48,256]{2,1,0:T(8,128)(2,1)S(1)}, u32[]{:S(2)}, u32[]{:S(2)}) async-start(bf16[16,48,256]{2,1,0:T(8,128)(2,1)} %get-tuple-element.8), calls=%async_computation.1 | async-start | bytes 786432 | tf_op jit(solution)/shard_map/all_to_all | solution.py:372
where the time goes:
time: 118 us; the launch traced here: 117 us
  starting transfers between devices  53.5 us (45%)
  waiting for transfers between devices  36.7 us (31%)
  blocking collectives  15.1 us (13%)
  Pallas kernels  9.15 us (8%)
  local copies, waits for them, and re-layouts  1.47 us (1%)
  between operations  1.47 us (1%)
    ppermute x1, starting transfers between devices, local(): pack = lax.ppermute(pack, 'tp', SWAP)  43.4 us
    all_to_all x1, waiting for transfers between devices, local(): ours = lax.all_to_all(copies, 'kv', split_axis=0, concat_axis=0, tiled=True)  19.4 us
    all_to_all x1, waiting for transfers between devices, local(): lax.all_to_all(partial, 'kv', split_axis=0, concat_axis=0, tiled=True)  17.3 us
    all_gather x1, blocking collectives, local(): lax.all_gather(total, 'tp', axis=0)  8.98 us
    all_to_all x1, starting transfers between devices, local(): lax.all_to_all(partial, 'kv', split_axis=0, concat_axis=0, tiled=True)  6.15 us
    all_gather x1, blocking collectives, local(): gathered = lax.all_gather(ours, 'tp', axis=0)  6.1 us
    pallas_call x1, Pallas kernels, local(): pl.pallas_call(layer_kernel, out_shape=(jax.ShapeDtypeStruct((kv, n, colu...  5.11 us
    pallas_call x1, Pallas kernels, local(): commit(state.reshape(seqs, rows, width), prev_keys.reshape(seqs * steps,...  4.04 us
  transfers between devices with their start and end apart: 3, of which 2 were waited for; matrix products, arithmetic and copies ran while one was open for 1% of the time, Pallas kernels for 0%

commit v1 on v0

--- a/solution.py
+++ b/solution.py
@@ -161,8 +161,7 @@
     x_ref, gain_ref, wq_ref, wk_ref, wv_ref, wg_ref, decay_ref, beta_ref, rate_ref, hg_ref, committed_hbm, wo_ref, pack_hbm,
     out_ref, same_hbm, keep_ref, pack_ref, sems,
 ):
-    _, blocks, all_rows, lanes = x_ref.shape
-    n = all_rows // 2
+    blocks, _, n, lanes = x_ref.shape
     seqs, rows, width = keep_ref.shape
     steps = n // seqs
     heads = decay_ref.shape[0]
@@ -188,11 +187,10 @@
         fetch(pack_hbm.at[5 * rows :, :columns], pack_ref.at[5 * rows :, :columns]),
     ]
     out_copy = fetch(pack_hbm.at[4 * rows : 5 * rows], pack_ref.at[4 * rows : 5 * rows])
-    own_rows = pl.ds(pl.multiple_of(tp * n, n), n)
     squares = jnp.zeros((n, lanes), F32)
     for b in range(blocks):
         for c in range(2):
-            part = x_ref[c, b, own_rows, :].astype(F32)
+            part = x_ref[b, c].astype(F32)
             squares = squares + part * part
     scale = lax.rsqrt(jnp.sum(squares, axis=-1, keepdims=True) / features + EPS)
     mine = jnp.zeros((4 * rows, n), F32)
@@ -202,7 +200,7 @@
         if b % (blocks // cuts) == 0:
             weight_copies[b // (blocks // cuts)].wait()
         at = slice(b * 2 * lanes, (b + 1) * 2 * lanes)
-        pair = jnp.concatenate([x_ref[c, b, own_rows, :] for c in range(2)], axis=1).astype(F32)
+        pair = jnp.concatenate([x_ref[b, 0], x_ref[b, 1]], axis=1).astype(F32)
         gain = jnp.concatenate([gain_ref[2 * b : 2 * b + 1, :], gain_ref[2 * b + 1 : 2 * b + 2, :]], axis=1)
         normed = (pair * scale * gain).astype(BF16)
         w = jnp.concatenate([r[:, at] for r in (wq_ref, wk_ref, wv_ref, wg_ref)], axis=0)
@@ -297,8 +295,10 @@
     kv = lax.axis_size("kv")
     tp = lax.axis_index("tp")
 
-    copies = jnp.broadcast_to(tokens.reshape(1, seqs * steps, lanes), (kv, seqs * steps, lanes))
-    ours = lax.all_to_all(copies, "kv", split_axis=0, concat_axis=0, tiled=True)
+    both = lax.all_gather(tokens.reshape(seqs * steps, lanes), "tp", axis=0)
+    mine = lax.dynamic_slice_in_dim(both, tp * n, n, 1)
+    copies = jnp.broadcast_to(mine[None], (kv, *mine.shape))
+    gathered = lax.all_to_all(copies, "kv", split_axis=0, concat_axis=0, tiled=True)
     weights = [w.reshape(rows, features) for w in (w_query, w_key, w_value, w_gate)]
     w_own = w_out.reshape(rows, features)
     gain = head_gain.reshape(1, rows)
@@ -338,7 +338,6 @@
         w_own,
     )
     pack = lax.ppermute(pack, "tp", SWAP)
-    gathered = lax.all_gather(ours, "tp", axis=0)
     columns = features // kv
     partial, committed = pl.pallas_call(
         layer_kernel,

time: 118 us -> 121 us (1.025)
  starting transfers between devices: 53.5 us -> 58.3 us
    all_to_all x1, starting transfers between devices: 6.15 us -> 11 us  [local(): lax.all_to_all(partial, 'kv', split_axis=0, concat_axis=0, tiled=True)]
    all_to_all x1, waiting for transfers between devices: 19.4 us -> 18.1 us  [local(): lax.all_to_all(copies, 'kv', split_axis=0, concat_axis=0, tiled=True)]
where the time goes in v1:
time: 121 us; the launch traced here: 120 us
  starting transfers between devices  58.3 us (48%)
  waiting for transfers between devices  35.7 us (30%)
  blocking collectives  14.3 us (12%)
  Pallas kernels  9.14 us (8%)
  local copies, waits for them, and re-layouts  1.48 us (1%)
  between operations  1.48 us (1%)
    ppermute x1, starting transfers between devices, local(): pack = lax.ppermute(pack, 'tp', SWAP)  43.4 us
    all_to_all x1, waiting for transfers between devices, local(): lax.all_to_all(copies, 'kv', split_axis=0, concat_axis=0, tiled=True)  18.1 us
    all_to_all x1, waiting for transfers between devices, local(): lax.all_to_all(partial, 'kv', split_axis=0, concat_axis=0, tiled=True)  17.5 us
    all_to_all x1, starting transfers between devices, local(): lax.all_to_all(partial, 'kv', split_axis=0, concat_axis=0, tiled=True)  11 us
    all_gather x1, blocking collectives, local(): lax.all_gather(total, 'tp', axis=0)  8.74 us
    all_gather x1, blocking collectives, local(): both = lax.all_gather(tokens.reshape(seqs * steps, lanes), 'tp', axis=0)  5.59 us
    pallas_call x1, Pallas kernels, local(): pl.pallas_call(layer_kernel, out_shape=(jax.ShapeDtypeStruct((kv, n, colu...  5.1 us
    pallas_call x1, Pallas kernels, local(): commit(state.reshape(seqs, rows, width), prev_keys.reshape(seqs * steps,...  4.04 us
  transfers between devices with their start and end apart: 3, of which 2 were waited for; matrix products, arithmetic and copies ran while one was open for 1% of the time, Pallas kernels for 0%

profile of v1, /device:TPU:65, one launch (start us, length us, event | category | flops | bytes accessed | tf_op | source)
XLA Modules:
  0.0 120.5 jit_solution(12301577604603747381)
XLA Ops:
  0.6 0.0 copy-start.9
  0.6 0.0 copy-start
  0.7 0.0 copy-start.1
  0.7 0.0 copy-start.2
  0.7 0.0 copy-start.3
  0.7 0.0 copy-start.4
  0.7 0.0 copy-start.5
  0.7 0.0 copy-start.6
  0.7 0.0 copy-start.7
  0.7 0.0 copy-start.8
  0.7 4.0 %commit.1 = (f32[24,64,128]{2,1,0:T(8,128)}, bf16[384,4096]{1,0:T(8,128)(2,1)}) custom-call(f32[24,64,128]{2,1,0:T(8,128)} %bitcast.44, bf16[96,128]{1,0:T(8,128)(2,1)} %bitcast.45, bf16[96,64]{1,0:T(8,128)(2,1)} %bitcast.46, f32[4,24]{1,0:T(4,128)} %bitcast.47, f32[4,24]{1,0:T(4,128)} %bitcast.48, s32[1,24]{1,0:T(1,128)} %bitcast.49, f32[1,64]{1,0:T(1,128)} %bitcast.38, ...), custom_call_target="tpu_custom_call" | custom-call | flops 2000000000 | bytes 8000000 | tf_op jit(solution)/shard_map/commit/pallas_call | solution.py:329
  4.8 43.4 %collective-permute-start = (bf16[384,4096]{1,0:T(8,128)(2,1)}, bf16[384,4096]{1,0:T(8,128)(2,1)}, u32[]{:S(2)}, u32[]{:S(2)}) collective-permute-start(bf16[384,4096]{1,0:T(8,128)(2,1)} %get-tuple-element.7), channel_id=1, source_target_pairs={{0,1},{1,0},{2,3},{3,2},{4,5},{5,4},{6,7},{7,6},{8,9},{9,8},{10,11... | collective-permute-start | bytes 9437192 | tf_op jit(solution)/shard_map/ppermute | solution.py:340
  48.2 0.0 copy-done.9
  48.2 5.6 %all_gather.9 = bf16[2,96,128]{2,1,0:T(8,128)(2,1)S(1)} all-gather(bf16[1,96,128]{2,1,0:T(8,128)(2,1)S(1)} %bitcast.43), channel_id=1, replica_groups=mesh['grp'=2,'dp'=8,'kv'=16,'tp'=2] {'tp'}, dimensions={0}, use_global_device_ids=true | all-gather | bytes 73728 | tf_op jit(solution)/shard_map/all_gather | solution.py:298
  53.8 0.8 broadcast_in_dim.2
  54.6 4.0 %all-to-all-start = ((bf16[16,2,48,128]{3,2,1,0:T(8,128)(2,1)}), bf16[16,2,48,128]{3,2,1,0:T(8,128)(2,1)S(1)}, u32[]{:S(2)}, u32[]{:S(2)}) async-start(bf16[16,2,48,128]{3,2,1,0:T(8,128)(2,1)} %broadcast_in_dim.2), calls=%async_computation | async-start | bytes 786432 | tf_op jit(solution)/shard_map/all_to_all | solution.py:301
  59.2 18.1 %all-to-all-done.x_ref = bf16[16,2,48,128]{3,2,1,0:T(8,128)(2,1)S(1)} async-done(((bf16[16,2,48,128]{3,2,1,0:T(8,128)(2,1)}), bf16[16,2,48,128]{3,2,1,0:T(8,128)(2,1)S(1)}, u32[]{:S(2)}, u32[]{:S(2)}) %all-to-all-start) | async-done | bytes 393248 | tf_op jit(solution)/shard_map/all_to_all | solution.py:301
  77.4 0.0 collective-permute-done.pack_hbm
  77.4 0.0 copy-done
  77.4 0.0 copy-done.2
  77.4 0.0 copy-done.3
  77.4 0.0 copy-done.4
  77.4 0.0 copy-done.5
  77.4 0.0 copy-done.6
  77.4 0.0 copy-done.7
  77.5 0.0 copy-done.8
  77.5 5.1 %layer.1 = (bf16[16,48,256]{2,1,0:T(8,128)(2,1)}, f32[24,64,128]{2,1,0:T(8,128)}) custom-call(bf16[16,2,48,128]{3,2,1,0:T(8,128)(2,1)S(1)} %all-to-all-done.x_ref, f32[32,128]{1,0:T(8,128)S(1)} %bitcast.37, bf16[64,4096]{1,0:T(8,128)(2,1)S(1)} %bitcast.26, bf16[64,4096]{1,0:T(8,128)(2,1)S(1)} %bitcast.28, ...), custom_call_target="tpu_custom_call", output_to_operand_aliasing={{1}: (10, {})} | custom-call | flops 1000000000 | bytes 6000000 | tf_op jit(solution)/shard_map/layer/pallas_call | solution.py:342
  82.6 11.0 %all-to-all-start.1 = ((bf16[16,48,256]{2,1,0:T(8,128)(2,1)}), bf16[16,48,256]{2,1,0:T(8,128)(2,1)S(1)}, u32[]{:S(2)}, u32[]{:S(2)}) async-start(bf16[16,48,256]{2,1,0:T(8,128)(2,1)} %get-tuple-element.8), calls=%async_computation.1 | async-start | bytes 786432 | tf_op jit(solution)/shard_map/all_to_all | solution.py:371
  93.6 17.5 %all-to-all-done.1 = bf16[16,48,256]{2,1,0:T(8,128)(2,1)S(1)} async-done(((bf16[16,48,256]{2,1,0:T(8,128)(2,1)}), bf16[16,48,256]{2,1,0:T(8,128)(2,1)S(1)}, u32[]{:S(2)}, u32[]{:S(2)}) %all-to-all-start.1) | async-done | bytes 393248 | tf_op jit(solution)/shard_map/all_to_all | solution.py:371
  111.1 0.1 reduce_sum.12
  111.1 8.7 %all-gather = bf16[96,256]{1,0:T(8,128)(2,1)S(1)} all-gather(bf16[48,256]{1,0:T(8,128)(2,1)S(1)} %reduce_sum.12), channel_id=2, replica_groups=mesh['grp'=2,'dp'=8,'kv'=16,'tp'=2] {'tp'}, dimensions={0}, use_global_device_ids=true | all-gather | bytes 73728 | tf_op jit(solution)/shard_map/all_gather | solution.py:373
  119.9 0.6 constant_dynamic-slice_fusion
  (2 shorter events, 0.0 us)
Async XLA Ops:
  0.6 47.5 %copy-start.9 = (bf16[24,4,128]{2,1,0:T(4,128)(2,1)S(1)}, bf16[24,4,128]{2,1,0:T(4,128)(2,1)}, u32[]{:S(2)}) copy-start(bf16[24,4,128]{2,1,0:T(4,128)(2,1)} %param.17) | copy-start | bytes 73732
  0.6 76.7 %copy-start = (bf16[1,64,4096]{2,1,0:T(8,128)(2,1)S(1)}, bf16[1,64,4096]{2,1,0:T(8,128)(2,1)}, u32[]{:S(2)}) copy-start(bf16[1,64,4096]{2,1,0:T(8,128)(2,1)} %param.19) | copy-start | bytes 1572868
  0.7 76.7 %copy-start.1 = (bf16[1,64,4096]{2,1,0:T(8,128)(2,1)S(1)}, bf16[1,64,4096]{2,1,0:T(8,128)(2,1)}, u32[]{:S(2)}) copy-start(bf16[1,64,4096]{2,1,0:T(8,128)(2,1)} %param.20) | copy-start | bytes 1572868
  0.7 76.7 %copy-start.2 = (bf16[1,64,4096]{2,1,0:T(8,128)(2,1)S(1)}, bf16[1,64,4096]{2,1,0:T(8,128)(2,1)}, u32[]{:S(2)}) copy-start(bf16[1,64,4096]{2,1,0:T(8,128)(2,1)} %param.21) | copy-start | bytes 1572868
  0.7 76.7 %copy-start.3 = (bf16[1,64,4096]{2,1,0:T(8,128)(2,1)S(1)}, bf16[1,64,4096]{2,1,0:T(8,128)(2,1)}, u32[]{:S(2)}) copy-start(bf16[1,64,4096]{2,1,0:T(8,128)(2,1)} %param.22) | copy-start | bytes 1572868
  0.7 76.7 %copy-start.4 = (bf16[1,64,4096]{2,1,0:T(8,128)(2,1)S(1)}, bf16[1,64,4096]{2,1,0:T(8,128)(2,1)}, u32[]{:S(2)}) copy-start(bf16[1,64,4096]{2,1,0:T(8,128)(2,1)} %param.27) | copy-start | bytes 1572868
  0.7 76.7 %copy-start.5 = (bf16[4096,16]{0,1:T(8,128)(2,1)S(1)}, bf16[4096,16]{0,1:T(8,128)(2,1)}, u32[]{:S(2)}) copy-start(bf16[4096,16]{0,1:T(8,128)(2,1)} %param.23) | copy-start | bytes 393220
  0.7 76.7 %copy-start.6 = (bf16[4096,16]{0,1:T(8,128)(2,1)S(1)}, bf16[4096,16]{0,1:T(8,128)(2,1)}, u32[]{:S(2)}) copy-start(bf16[4096,16]{0,1:T(8,128)(2,1)} %param.24) | copy-start | bytes 393220
  0.7 76.7 %copy-start.7 = (f32[4096]{0:T(1024)S(1)}, f32[4096]{0:T(1024)}, u32[]{:S(2)}) copy-start(f32[4096]{0:T(1024)} %param.18) | copy-start | bytes 49156
  0.7 76.7 %copy-start.8 = (f32[64]{0:T(128)S(1)}, f32[64]{0:T(128)}, u32[]{:S(2)}) copy-start(f32[64]{0:T(128)} %param.26) | copy-start | bytes 772
  4.8 72.6 %collective-permute-start = (bf16[384,4096]{1,0:T(8,128)(2,1)}, bf16[384,4096]{1,0:T(8,128)(2,1)}, u32[]{:S(2)}, u32[]{:S(2)}) collective-permute-start(bf16[384,4096]{1,0:T(8,128)(2,1)} %get-tuple-element.7), channel_id=1, source_target_pairs={{0,1},{1,0},{2,3},{3,2},{4,5},{5,4},{6,7},{7,6},{8,9},{9,8},{10,11... | collective-permute-start | bytes 9437192 | tf_op jit(solution)/shard_map/ppermute | solution.py:340
  54.6 22.8 %all-to-all-start = ((bf16[16,2,48,128]{3,2,1,0:T(8,128)(2,1)}), bf16[16,2,48,128]{3,2,1,0:T(8,128)(2,1)S(1)}, u32[]{:S(2)}, u32[]{:S(2)}) async-start(bf16[16,2,48,128]{3,2,1,0:T(8,128)(2,1)} %broadcast_in_dim.2), calls=%async_computation | async-start | bytes 786432 | tf_op jit(solution)/shard_map/all_to_all | solution.py:301
  82.6 28.5 %all-to-all-start.1 = ((bf16[16,48,256]{2,1,0:T(8,128)(2,1)}), bf16[16,48,256]{2,1,0:T(8,128)(2,1)S(1)}, u32[]{:S(2)}, u32[]{:S(2)}) async-start(bf16[16,48,256]{2,1,0:T(8,128)(2,1)} %get-tuple-element.8), calls=%async_computation.1 | async-start | bytes 786432 | tf_op jit(solution)/shard_map/all_to_all | solution.py:371

commit v2 on v1

--- a/solution.py
+++ b/solution.py
@@ -295,6 +295,8 @@
     kv = lax.axis_size("kv")
     tp = lax.axis_index("tp")
 
+    first = tp == 0
+    first, tokens = lax.optimization_barrier((first, tokens))
     both = lax.all_gather(tokens.reshape(seqs * steps, lanes), "tp", axis=0)
     mine = lax.dynamic_slice_in_dim(both, tp * n, n, 1)
     copies = jnp.broadcast_to(mine[None], (kv, *mine.shape))
@@ -370,7 +372,8 @@
     )
     parts = lax.all_to_all(partial, "kv", split_axis=0, concat_axis=0, tiled=True)
     total = parts.astype(F32).sum(axis=0).astype(BF16)
-    mixed = lax.dynamic_slice_in_dim(lax.all_gather(total, "tp", axis=0), tp * lanes, lanes, 2)
+    joined = lax.all_gather(total, "tp", axis=0)
+    mixed = jnp.where(first, joined[:, :, :lanes], joined[:, :, lanes:])
     return mixed.reshape(seqs, steps, lanes), committed.reshape(state.shape)
 
 

time: 121 us -> 120 us (level)
  blocking collectives: 14.3 us -> 42.6 us
  waiting for transfers between devices: 35.7 us -> 18.1 us
  starting transfers between devices: 58.3 us -> 47.4 us
    all_to_all x0 -> x1, blocking collectives: none -> 28.3 us  [local(): lax.all_to_all(partial, 'kv', split_axis=0, concat_axis=0, tiled=True)]
    all_to_all x1 -> x0, waiting for transfers between devices: 17.5 us -> none  [local(): lax.all_to_all(partial, 'kv', split_axis=0, concat_axis=0, tiled=True)]
    all_to_all x1 -> x0, starting transfers between devices: 11 us -> none  [local(): lax.all_to_all(partial, 'kv', split_axis=0, concat_axis=0, tiled=True)]
  transfers between devices with their start and end apart: 3 -> 2, of which waited for: 2 -> 1; matrix products, arithmetic and copies ran while one was open for 1% -> 1% of each run, Pallas kernels for 0% -> 0%
where the time goes in v2:
time: 120 us; the launch traced here: 119 us
  starting transfers between devices  47.4 us (40%)
  blocking collectives  42.6 us (36%)
  waiting for transfers between devices  18.1 us (15%)
  Pallas kernels  8.36 us (7%)
  between operations  1.47 us (1%)
    ppermute x1, starting transfers between devices, local(): pack = lax.ppermute(pack, 'tp', SWAP)  43.4 us
    all_to_all x1, blocking collectives, local(): lax.all_to_all(partial, 'kv', split_axis=0, concat_axis=0, tiled=True)  28.3 us
    all_to_all x1, waiting for transfers between devices, local(): lax.all_to_all(copies, 'kv', split_axis=0, concat_axis=0, tiled=True)  18.1 us
    all_gather x1, blocking collectives, local(): joined = lax.all_gather(total, 'tp', axis=0)  8.71 us
    all_gather x1, blocking collectives, local(): both = lax.all_gather(tokens.reshape(seqs * steps, lanes), 'tp', axis=0)  5.59 us
    pallas_call x1, Pallas kernels, local(): pl.pallas_call(layer_kernel, out_shape=(jax.ShapeDtypeStruct((kv, n, colu...  4.33 us
    pallas_call x1, Pallas kernels, local(): commit(state.reshape(seqs, rows, width), prev_keys.reshape(seqs * steps,...  4.03 us
    all_to_all x1, starting transfers between devices, local(): lax.all_to_all(copies, 'kv', split_axis=0, concat_axis=0, tiled=True)  3.99 us
  transfers between devices with their start and end apart: 2, of which 1 were waited for; matrix products, arithmetic and copies ran while one was open for 1% of the time, Pallas kernels for 0%

profile of v2, /device:TPU:65, one launch (start us, length us, event | category | flops | bytes accessed | tf_op | source)
XLA Modules:
  0.0 119.5 jit_solution(3308880071010312573)
XLA Ops:
  0.6 0.0 copy-start.9
  0.6 0.0 copy-start
  0.7 0.0 copy-start.1
  0.7 0.0 copy-start.2
  0.7 0.0 copy-start.3
  0.7 0.0 copy-start.4
  0.7 0.0 copy-start.5
  0.7 0.0 copy-start.6
  0.7 0.0 copy-start.7
  0.7 0.0 copy-start.8
  0.7 4.0 %commit.1 = (f32[24,64,128]{2,1,0:T(8,128)}, bf16[384,4096]{1,0:T(8,128)(2,1)}) custom-call(f32[24,64,128]{2,1,0:T(8,128)} %bitcast.44, bf16[96,128]{1,0:T(8,128)(2,1)} %bitcast.45, bf16[96,64]{1,0:T(8,128)(2,1)} %bitcast.46, f32[4,24]{1,0:T(4,128)} %bitcast.47, f32[4,24]{1,0:T(4,128)} %bitcast.48, s32[1,24]{1,0:T(1,128)} %bitcast.49, f32[1,64]{1,0:T(1,128)} %bitcast.38, ...), custom_call_target="tpu_custom_call" | custom-call | flops 2000000000 | bytes 8000000 | tf_op jit(solution)/shard_map/commit/pallas_call | solution.py:331
  4.8 43.4 %collective-permute-start = (bf16[384,4096]{1,0:T(8,128)(2,1)}, bf16[384,4096]{1,0:T(8,128)(2,1)}, u32[]{:S(2)}, u32[]{:S(2)}) collective-permute-start(bf16[384,4096]{1,0:T(8,128)(2,1)} %get-tuple-element.11), channel_id=1, source_target_pairs={{0,1},{1,0},{2,3},{3,2},{4,5},{5,4},{6,7},{7,6},{8,9},{9,8},{10,11... | collective-permute-start | bytes 9437192 | tf_op jit(solution)/shard_map/ppermute | solution.py:342
  48.2 0.0 copy-done.9
  48.2 5.6 %all_gather.9 = bf16[2,96,128]{2,1,0:T(8,128)(2,1)S(1)} all-gather(bf16[1,96,128]{2,1,0:T(8,128)(2,1)S(1)} %bitcast.42), channel_id=1, replica_groups=mesh['grp'=2,'dp'=8,'kv'=16,'tp'=2] {'tp'}, dimensions={0}, use_global_device_ids=true | all-gather | bytes 73728 | tf_op jit(solution)/shard_map/all_gather | solution.py:300
  53.8 0.8 broadcast_in_dim.2
  54.6 4.0 %all-to-all-start = ((bf16[16,2,48,128]{3,2,1,0:T(8,128)(2,1)}), bf16[16,2,48,128]{3,2,1,0:T(8,128)(2,1)S(1)}, u32[]{:S(2)}, u32[]{:S(2)}) async-start(bf16[16,2,48,128]{3,2,1,0:T(8,128)(2,1)} %broadcast_in_dim.2), calls=%async_computation | async-start | bytes 786432 | tf_op jit(solution)/shard_map/all_to_all | solution.py:303
  59.2 18.1 %all-to-all-done.x_ref = bf16[16,2,48,128]{3,2,1,0:T(8,128)(2,1)S(1)} async-done(((bf16[16,2,48,128]{3,2,1,0:T(8,128)(2,1)}), bf16[16,2,48,128]{3,2,1,0:T(8,128)(2,1)S(1)}, u32[]{:S(2)}, u32[]{:S(2)}) %all-to-all-start) | async-done | bytes 393248 | tf_op jit(solution)/shard_map/all_to_all | solution.py:303
  77.4 0.0 collective-permute-done.pack_hbm
  77.4 0.0 copy-done
  77.4 0.0 copy-done.1
  77.4 0.0 copy-done.2
  77.4 0.0 copy-done.3
  77.4 0.0 copy-done.4
  77.4 0.0 copy-done.5
  77.4 0.0 copy-done.6
  77.4 0.0 copy-done.7
  77.4 0.0 copy-done.8
  77.5 4.3 %layer.1 = (bf16[16,48,256]{2,1,0:T(8,128)(2,1)S(1)}, f32[24,64,128]{2,1,0:T(8,128)}) custom-call(bf16[16,2,48,128]{3,2,1,0:T(8,128)(2,1)S(1)} %all-to-all-done.x_ref, f32[32,128]{1,0:T(8,128)S(1)} %bitcast.37, bf16[64,4096]{1,0:T(8,128)(2,1)S(1)} %bitcast.26, bf16[64,4096]{1,0:T(8,128)(2,1)S(1)} %bitcast.28, ...), custom_call_target="tpu_custom_call", output_to_operand_aliasing={{1}: (10, {})} | custom-call | flops 1000000000 | bytes 6000000 | tf_op jit(solution)/shard_map/layer/pallas_call | solution.py:344
  81.8 28.3 %all_to_all.10 = bf16[16,48,256]{2,1,0:T(8,128)(2,1)S(1)} all-to-all(bf16[16,48,256]{2,1,0:T(8,128)(2,1)S(1)} %get-tuple-element.12), channel_id=1, replica_groups=mesh['grp'=2,'dp'=8,'kv'=16,'tp'=2] {'kv'}, dimensions={0} | all-to-all | bytes 786432 | tf_op jit(solution)/shard_map/all_to_all | solution.py:373
  110.1 0.1 reduce_sum.12
  110.1 8.7 %all-gather = bf16[96,256]{1,0:T(8,128)(2,1)S(1)} all-gather(bf16[48,256]{1,0:T(8,128)(2,1)S(1)} %reduce_sum.12), channel_id=2, replica_groups=mesh['grp'=2,'dp'=8,'kv'=16,'tp'=2] {'tp'}, dimensions={0}, use_global_device_ids=true | all-gather | bytes 73728 | tf_op jit(solution)/shard_map/all_gather | solution.py:375
  118.9 0.6 slice_select_fusion
  (1 shorter events, 0.0 us)
Async XLA Ops:
  0.6 47.5 %copy-start.9 = (bf16[24,4,128]{2,1,0:T(4,128)(2,1)S(1)}, bf16[24,4,128]{2,1,0:T(4,128)(2,1)}, u32[]{:S(2)}) copy-start(bf16[24,4,128]{2,1,0:T(4,128)(2,1)} %param.17) | copy-start | bytes 73732
  0.6 76.7 %copy-start = (bf16[1,64,4096]{2,1,0:T(8,128)(2,1)S(1)}, bf16[1,64,4096]{2,1,0:T(8,128)(2,1)}, u32[]{:S(2)}) copy-start(bf16[1,64,4096]{2,1,0:T(8,128)(2,1)} %param.19) | copy-start | bytes 1572868
  0.7 76.7 %copy-start.1 = (bf16[1,64,4096]{2,1,0:T(8,128)(2,1)S(1)}, bf16[1,64,4096]{2,1,0:T(8,128)(2,1)}, u32[]{:S(2)}) copy-start(bf16[1,64,4096]{2,1,0:T(8,128)(2,1)} %param.20) | copy-start | bytes 1572868
  0.7 76.7 %copy-start.2 = (bf16[1,64,4096]{2,1,0:T(8,128)(2,1)S(1)}, bf16[1,64,4096]{2,1,0:T(8,128)(2,1)}, u32[]{:S(2)}) copy-start(bf16[1,64,4096]{2,1,0:T(8,128)(2,1)} %param.21) | copy-start | bytes 1572868
  0.7 76.7 %copy-start.3 = (bf16[1,64,4096]{2,1,0:T(8,128)(2,1)S(1)}, bf16[1,64,4096]{2,1,0:T(8,128)(2,1)}, u32[]{:S(2)}) copy-start(bf16[1,64,4096]{2,1,0:T(8,128)(2,1)} %param.22) | copy-start | bytes 1572868
  0.7 76.7 %copy-start.4 = (bf16[1,64,4096]{2,1,0:T(8,128)(2,1)S(1)}, bf16[1,64,4096]{2,1,0:T(8,128)(2,1)}, u32[]{:S(2)}) copy-start(bf16[1,64,4096]{2,1,0:T(8,128)(2,1)} %param.27) | copy-start | bytes 1572868
  0.7 76.7 %copy-start.5 = (bf16[4096,16]{0,1:T(8,128)(2,1)S(1)}, bf16[4096,16]{0,1:T(8,128)(2,1)}, u32[]{:S(2)}) copy-start(bf16[4096,16]{0,1:T(8,128)(2,1)} %param.23) | copy-start | bytes 393220
  0.7 76.7 %copy-start.6 = (bf16[4096,16]{0,1:T(8,128)(2,1)S(1)}, bf16[4096,16]{0,1:T(8,128)(2,1)}, u32[]{:S(2)}) copy-start(bf16[4096,16]{0,1:T(8,128)(2,1)} %param.24) | copy-start | bytes 393220
  0.7 76.7 %copy-start.7 = (f32[4096]{0:T(1024)S(1)}, f32[4096]{0:T(1024)}, u32[]{:S(2)}) copy-start(f32[4096]{0:T(1024)} %param.18) | copy-start | bytes 49156
  0.7 76.7 %copy-start.8 = (f32[64]{0:T(128)S(1)}, f32[64]{0:T(128)}, u32[]{:S(2)}) copy-start(f32[64]{0:T(128)} %param.26) | copy-start | bytes 772
  4.8 72.6 %collective-permute-start = (bf16[384,4096]{1,0:T(8,128)(2,1)}, bf16[384,4096]{1,0:T(8,128)(2,1)}, u32[]{:S(2)}, u32[]{:S(2)}) collective-permute-start(bf16[384,4096]{1,0:T(8,128)(2,1)} %get-tuple-element.11), channel_id=1, source_target_pairs={{0,1},{1,0},{2,3},{3,2},{4,5},{5,4},{6,7},{7,6},{8,9},{9,8},{10,11... | collective-permute-start | bytes 9437192 | tf_op jit(solution)/shard_map/ppermute | solution.py:342
  54.6 22.8 %all-to-all-start = ((bf16[16,2,48,128]{3,2,1,0:T(8,128)(2,1)}), bf16[16,2,48,128]{3,2,1,0:T(8,128)(2,1)S(1)}, u32[]{:S(2)}, u32[]{:S(2)}) async-start(bf16[16,2,48,128]{3,2,1,0:T(8,128)(2,1)} %broadcast_in_dim.2), calls=%async_computation | async-start | bytes 786432 | tf_op jit(solution)/shard_map/all_to_all | solution.py:303
